TPU v7x, 32 devices: a whole 2x2x4 slice. The times are simulated.
32 devices in a mesh: grp: 2 (over y), fs: 4 (over z), tp: 4 (over x, core).
Axes of the slice: x: 2, y: 2, z: 4, core: 2. Of those that a mesh axis runs over, the one named last changes fastest.
Arguments:
- tokens: bfloat16 [1024, 2048], P(('grp', 'fs')), parts along dimension 0, may hold values from -12 to 12, as said below
- mix_heads: bfloat16 [1024, 2048], P(('grp', 'fs'), 'tp'), parts along dimension 0, may hold values from -6 to 6
- norm_first: float32 [2048], replicated, may hold values from 0.1 to 1.9
- gate_first: bfloat16 [2048, 5632], P('fs', 'tp'), may hold values from -0.125 to 0.125
- up_first: bfloat16 [2048, 5632], P('fs', 'tp'), may hold values from -0.125 to 0.125
- down_first: bfloat16 [5632, 2048], P('tp', 'fs'), may hold values from -0.078125 to 0.078125
- out_weight: bfloat16 [2048, 2048], P('tp', 'fs'), may hold values from -0.125 to 0.125
- norm_second: float32 [2048], replicated, may hold values from 0.1 to 1.9
- gate_second: bfloat16 [2048, 5632], P('fs', 'tp'), may hold values from -0.125 to 0.125
- up_second: bfloat16 [2048, 5632], P('fs', 'tp'), may hold values from -0.125 to 0.125
- down_second: bfloat16 [5632, 2048], P('tp', 'fs'), may hold values from -0.078125 to 0.078125
Outputs:
- layer_out: bfloat16 [1024, 2048], P(('grp', 'fs')), parts along dimension 0
There are 2 independent parts, one for each index of `grp`. A program takes and returns all parts, laid end to end along the dimension named above; an argument that names none is the same for every part. Nothing has to cross between parts.
Inputs may be any that keep to these rules, and one draw needn't show every extreme that they name: Each row of tokens carries a scale of its own.
All inputs are finite; a program needn't handle non-finite values.
Results may differ from a plain program's by a relative error of at most 0.014.
Values may be sent and summed in bfloat16 or wider, within the bound.
A program may use at most 64 MiB of HBM per device.

v0:
```python
import functools

import jax
import jax.numpy as jnp
from jax import lax
from jax.experimental import pallas as pl
from jax.experimental.pallas import tpu as pltpu
from jax.sharding import PartitionSpec as P

EPS = 0.1
MESH = pl.DeviceIdType.MESH
BF16 = jnp.bfloat16
F32 = jnp.float32


def loop(count, body):
    def step(i, carry):
        body(i)
        return carry

    lax.fori_loop(0, count, step, 0)


def kernel(n_fs, n_tp, chunk,
           tok, mix, gain1, wg1, wu1, wd1, wo, gain2, wg2, wu2, wd2,
           out,
           vg1, vu1, vd1, vo, vg2, vu2, vd2,
           raw, nb2, mixed, grads, sums, in1, in2, hid1, hid2,
           terms, got1, got2, resid, squares1, squares, done_rows, joined,
           wsem, p0_send, p0_recv, fw_send, fw_recv, s1_send, s1_recv, mix_send, mix_recv,
           rs_send, rs_recv, ag_send, ag_recv, tp_send, tp_recv,
           sq_send, sq_recv, nrm_send, nrm_recv, nfw_send, nfw_recv,
           out_send, out_recv, ofw_send, ofw_recv):
    f, t = lax.axis_index("fs"), lax.axis_index("tp")
    rows_in, width = tok.shape
    total = rows_in * n_fs
    share = total // n_tp
    half = total // 2
    n_chunks = half // chunk
    dc = width // n_fs

    weights = ((wg1, vg1), (wu1, vu1), (wd1, vd1), (wo, vo), (wg2, vg2), (wu2, vu2), (wd2, vd2))
    loads = [pltpu.make_async_copy(a, b, wsem.at[i]) for i, (a, b) in enumerate(weights)]
    for load in loads:
        load.start()

    barrier = pltpu.get_barrier_semaphore()

    def greet(i):
        pf, pt = i // n_tp, i % n_tp

        @pl.when(jnp.logical_or(pf != f, pt != t))
        def _():
            pl.semaphore_signal(barrier, inc=1, device_id={"fs": pf, "tp": pt}, device_id_type=MESH)

    loop(n_fs * n_tp, greet)

    def cols(j):
        return pl.ds(pl.multiple_of(j * dc, dc), dc)

    def block(j, size):
        return pl.ds(pl.multiple_of(j * size, size), size)

    def remote(src, dst, send, recv, **where):
        return pltpu.make_async_remote_copy(
            src_ref=src, dst_ref=dst, send_sem=send, recv_sem=recv,
            device_id=where, device_id_type=MESH)

    c_own = t % 2
    partner = t + 1 - 2 * c_own
    half_in = rows_in // 2
    n_pairs = n_tp // 2

    def squares_of(x):
        own = jnp.sum(x * x, axis=-1, keepdims=True)
        return jnp.transpose(jnp.broadcast_to(own, (x.shape[0], 128)))[0:8, :]

    def scale_of(summed):
        column = jnp.transpose(jnp.broadcast_to(summed[0:1, :], (128, summed.shape[1])))[:, 0:1]
        return lax.rsqrt(column * (1.0 / width) + EPS)

    def piece_of(slot):
        return pl.ds(pl.multiple_of(slot * rows_in + c_own * half_in, half_in), half_in)

    def p0_copy(j, slot):
        return remote(tok.at[block(c_own, half_in), cols(j)], raw.at[piece_of(slot), :],
                      p0_send.at[j], p0_recv.at[slot], fs=j)

    def fw_copy(slot):
        place = raw.at[piece_of(slot), :]
        return remote(place, place, fw_send.at[slot], fw_recv.at[slot], tp=partner)

    def s1_copy(j, slot):
        return remote(squares1.at[f], squares1.at[slot], s1_send.at[j], s1_recv.at[slot], fs=j)

    def sq_copy(j, slot):
        return remote(squares.at[f], squares.at[slot], sq_send.at[j], sq_recv.at[slot], fs=j)

    def mix_copy(slot, side, where):
        place = mixed.at[block(slot, rows_in), :]
        return remote(place, place, mix_send.at[slot, side], mix_recv.at[slot], fs=where)

    mixed[block(f, rows_in), :] = mix[...]
    pl.semaphore_wait(barrier, n_fs * n_tp - 1)

    def p0_start(i):
        p0_copy((f + 1 + i) % n_fs, f).start()

    loop(n_fs - 1, p0_start)
    squares1[f] = squares_of(tok[...].astype(F32))

    def s1_start(i):
        s1_copy((f + 1 + i) % n_fs, f).start()

    loop(n_fs - 1, s1_start)

    @pl.when(f < n_fs - 1)
    def _():
        mix_copy(f, 0, f + 1).start()

    @pl.when(f > 0)
    def _():
        mix_copy(f, 1, f - 1).start()

    raw[block(f, rows_in), :] = tok[:, cols(f)]

    def gates_one(j):
        rows = block(j, rows_in)
        x = (raw[rows, :].astype(F32) * scale_of(squares1[j]) * gain1[:, cols(f)]).astype(BF16)
        grads[0, rows, :] = jnp.dot(x, vg1[...], preferred_element_type=F32)
        grads[1, rows, :] = jnp.dot(x, vu1[...], preferred_element_type=F32)

    def side_of(side):
        hops = jnp.where(side == 0, n_fs - 1 - f, f)
        toward = jnp.where(side == 0, f - 1, f + 1)
        away = jnp.where(side == 0, f + 1, f - 1)
        return hops, toward, away

    near = jnp.where(2 * f >= n_fs, 0, 1)

    def chain(layer, arrived, hid, with_mix):
        def rows_of(side, c):
            return pl.ds(pl.multiple_of(side * half + c * chunk, chunk), chunk)

        def rs_copy(side, c, where):
            rows = rows_of(side, c)
            return remote(sums.at[:, rows, :], arrived.at[:, rows, :],
                          rs_send.at[layer, side, c], rs_recv.at[layer, side, c], fs=where)

        def ag_copy(side, c, where):
            rows = rows_of(side, c)
            return remote(hid.at[rows, :], hid.at[rows, :],
                          ag_send.at[layer, side, c], ag_recv.at[layer, side, c], fs=where)

        for side in (0, 1):
            hops, toward, away = side_of(side)

            @pl.when(hops == 0)
            def _():
                def first(c):
                    rows = rows_of(side, c)
                    sums[:, rows, :] = grads[:, rows, :].astype(BF16)
                    rs_copy(side, c, toward).start()

                loop(n_chunks, first)

        def step(s):
            for k in (0, 1):
                side = near if k == 0 else 1 - near
                hops, toward, away = side_of(side)
                c = s - hops

                @pl.when(jnp.logical_and(hops > 0, jnp.logical_and(c >= 0, c < n_chunks)))
                def _():
                    rows = rows_of(side, c)
                    rs_copy(side, c, f).wait_recv()

                    @pl.when(hops < n_fs - 1)
                    def _():
                        sums[:, rows, :] = (grads[:, rows, :] + arrived[:, rows, :].astype(F32)).astype(BF16)
                        rs_copy(side, c, toward).start()

                    @pl.when(hops == n_fs - 1)
                    def _():
                        g = grads[0, rows, :] + arrived[0, rows, :].astype(F32)
                        v = grads[1, rows, :] + arrived[1, rows, :].astype(F32)
                        hid[rows, :] = (g / (1.0 + jnp.exp(-g)) * v).astype(BF16)
                        ag_copy(side, c, away).start()

            if with_mix:
                @pl.when(jnp.logical_and(s > 0, s < n_fs))
                def _():
                    low, high = f - s, f + s

                    @pl.when(low >= 0)
                    def _():
                        mix_copy(low, 0, f).wait_recv()

                        @pl.when(f < n_fs - 1)
                        def _():
                            mix_copy(low, 0, f + 1).start()

                    @pl.when(high < n_fs)
                    def _():
                        mix_copy(high, 1, f).wait_recv()

                        @pl.when(f > 0)
                        def _():
                            mix_copy(high, 1, f - 1).start()

        loop(n_chunks + n_fs - 1, step)

        def relay(c):
            for k in (0, 1):
                side = 1 - near if k == 0 else near
                hops, toward, away = side_of(side)

                @pl.when(hops < n_fs - 1)
                def _():
                    ag_copy(side, c, f).wait_recv()

                    @pl.when(hops > 0)
                    def _():
                        ag_copy(side, c, away).start()

        def drain(c):
            for side in (0, 1):
                hops, toward, away = side_of(side)

                @pl.when(hops < n_fs - 1)
                def _():
                    rs_copy(side, c, f).wait_send()

                @pl.when(hops > 0)
                def _():
                    ag_copy(side, c, f).wait_send()

        return relay, lambda: loop(n_chunks, drain)

    def tp_copy(layer, j, slot, got):
        return remote(terms.at[block(j, share), :], got.at[slot],
                      tp_send.at[layer, j], tp_recv.at[layer, slot], tp=j)

    def down(layer, relay, hid, vd, got, with_mix):
        per_block = n_chunks // n_pairs

        def piece(b):
            def inner(i):
                relay(b * per_block + i)

            loop(per_block, inner)
            for side in (0, 1):
                j = side * n_pairs + b
                rows = block(j, share)
                value = 0.5 * jnp.dot(hid[rows, :], vd[...], preferred_element_type=F32)
                if with_mix:
                    value = value + jnp.dot(mixed[rows, :], vo[...], preferred_element_type=F32)
                terms[rows, :] = value.astype(BF16)

                @pl.when(j != t)
                def _():
                    tp_copy(layer, j, t, got).start()

        loop(n_pairs, piece)

    def reduce_tp(layer, got, start_value):
        resid[...] = start_value + terms[block(t, share), :].astype(F32)

        def add(i):
            j = (t + 1 + i) % n_tp
            tp_copy(layer, j, j, got).wait_recv()
            resid[...] = resid[...] + got[j].astype(F32)

        loop(n_tp - 1, add)

        def drain(i):
            j = (t + 1 + i) % n_tp
            tp_copy(layer, j, t, got).wait_send()

        loop(n_tp - 1, drain)

    loads[0].wait()
    loads[1].wait()
    gates_one(f)

    def pass_on(i):
        j = (f + 1 + i) % n_fs
        p0_copy(j, j).wait_recv()
        fw_copy(j).start()

    loop(n_fs - 1, pass_on)

    def other_rows(i):
        j = (f + 1 + i) % n_fs
        s1_copy(j, j).wait_recv()
        fw_in(j).wait_recv()
        gates_one(j)

    def fw_in(slot):
        start = pl.multiple_of(slot * rows_in + (1 - c_own) * half_in, half_in)
        place = raw.at[pl.ds(start, half_in), :]
        return remote(place, place, fw_send.at[slot], fw_recv.at[slot], tp=partner)

    loop(n_fs - 1, other_rows)
    relay_one, drain_one = chain(0, in1, hid1, True)
    loads[2].wait()
    loads[3].wait()
    down(0, relay_one, hid1, vd1, got1, True)
    reduce_tp(0, got1, raw[block(t, share), :].astype(F32))

    squares[f] = squares_of(resid[...])

    def sq_start(i):
        sq_copy((f + 1 + i) % n_fs, f).start()

    def sq_wait(i):
        j = (f + 1 + i) % n_fs
        sq_copy(j, j).wait_recv()

    loop(n_fs - 1, sq_start)
    drain_one()
    loop(n_fs - 1, sq_wait)
    summed = squares[0]
    for j in range(1, n_fs):
        summed = summed + squares[j]
    nb2[block(t, share), :] = (resid[...] * scale_of(summed) * gain2[:, cols(f)]).astype(BF16)

    def nrm_copy(j, slot):
        place = nb2.at[block(slot, share), :]
        return remote(place, place, nrm_send.at[j], nrm_recv.at[slot], tp=j)

    def nfw_copy(slot):
        place = nb2.at[block(slot, share), :]
        return remote(place, place, nfw_send.at[slot], nfw_recv.at[slot], tp=partner)

    def same_core(i):
        return (t + 2 + 2 * i) % n_tp

    def nrm_start(i):
        nrm_copy(same_core(i), t).start()

    loop(n_pairs - 1, nrm_start)
    nfw_copy(t).start()
    loads[4].wait()
    loads[5].wait()

    def gates_two(j):
        rows = block(j, share)
        x = nb2[rows, :]
        grads[0, rows, :] = jnp.dot(x, vg2[...], preferred_element_type=F32)
        grads[1, rows, :] = jnp.dot(x, vu2[...], preferred_element_type=F32)

    gates_two(t)
    nfw_copy(partner).wait_recv()
    gates_two(partner)

    def nrm_pass(i):
        j = same_core(i)
        nrm_copy(j, j).wait_recv()
        nfw_copy(j).start()
        gates_two(j)

    loop(n_pairs - 1, nrm_pass)

    def nrm_last(i):
        j = (partner + 2 + 2 * i) % n_tp
        nfw_copy(j).wait_recv()
        gates_two(j)

    loop(n_pairs - 1, nrm_last)
    relay_two, drain_two = chain(1, in2, hid2, False)
    loads[6].wait()
    down(1, relay_two, hid2, vd2, got2, False)
    reduce_tp(1, got2, resid[...])
    done_rows[...] = resid[...].astype(BF16)

    def out_copy(j, slot):
        return remote(done_rows, joined.at[:, cols(slot)], out_send.at[j], out_recv.at[slot], fs=t, tp=j)

    def ofw_copy(slot):
        place = joined.at[:, cols(slot)]
        return remote(place, place, ofw_send.at[slot], ofw_recv.at[slot], tp=partner)

    def out_start(i):
        j = c_own + 2 * i

        @pl.when(jnp.logical_or(f != t, j != t))
        def _():
            out_copy(j, f).start()

    loop(n_pairs, out_start)

    @pl.when(f == t)
    def _():
        joined[:, cols(f)] = done_rows[...]

    takes = c_own == f % 2

    @pl.when(takes)
    def _():
        def take(i):
            j = (f + i) % n_fs

            @pl.when(jnp.logical_or(f != t, j != f))
            def _():
                out_copy(t, j).wait_recv()

            ofw_copy(j).start()

        loop(n_fs, take)

    @pl.when(jnp.logical_not(takes))
    def _():
        def take(i):
            ofw_copy((f + i) % n_fs).wait_recv()

        loop(n_fs, take)

    out[...] = joined[...]

    drain_two()

    def last_fs(i):
        j = (f + 1 + i) % n_fs
        p0_copy(j, f).wait_send()
        fw_copy(j).wait_send()
        s1_copy(j, f).wait_send()
        sq_copy(j, f).wait_send()

    loop(n_fs - 1, last_fs)

    def last_mix(j):
        @pl.when(jnp.logical_and(j <= f, f < n_fs - 1))
        def _():
            mix_copy(j, 0, f).wait_send()

        @pl.when(jnp.logical_and(j >= f, f > 0))
        def _():
            mix_copy(j, 1, f).wait_send()

        @pl.when(takes)
        def _():
            ofw_copy(j).wait_send()

    loop(n_fs, last_mix)

    def last_nrm(i):
        nrm_copy(same_core(i), t).wait_send()

    loop(n_pairs - 1, last_nrm)

    def last_out(i):
        j = c_own + 2 * i
        nfw_copy(j).wait_send()

        @pl.when(jnp.logical_or(f != t, j != t))
        def _():
            out_copy(j, f).wait_send()

    loop(n_pairs, last_out)


def solution(mesh):
    n_fs, n_tp = mesh.shape["fs"], mesh.shape["tp"]

    def local(tokens, mix_heads, norm_first, gate_first, up_first, down_first, out_weight,
              norm_second, gate_second, up_second, down_second):
        rows_in, width = tokens.shape
        total = rows_in * n_fs
        share = total // n_tp
        dc, hidden = gate_first.shape
        heads = mix_heads.shape[1]
        chunk = rows_in // 2
        n_chunks = total // 2 // chunk
        dma = pltpu.SemaphoreType.DMA
        vmem = pl.BlockSpec(memory_space=pltpu.VMEM)
        hbm = pl.BlockSpec(memory_space=pl.ANY)
        return pl.pallas_call(
            functools.partial(kernel, n_fs, n_tp, chunk),
            out_shape=jax.ShapeDtypeStruct((rows_in, width), BF16),
            in_specs=[vmem, vmem, vmem, hbm, hbm, hbm, hbm, vmem, hbm, hbm, hbm],
            out_specs=vmem,
            scratch_shapes=[
                pltpu.VMEM(gate_first.shape, BF16),
                pltpu.VMEM(up_first.shape, BF16),
                pltpu.VMEM(down_first.shape, BF16),
                pltpu.VMEM(out_weight.shape, BF16),
                pltpu.VMEM(gate_second.shape, BF16),
                pltpu.VMEM(up_second.shape, BF16),
                pltpu.VMEM(down_second.shape, BF16),
                pltpu.VMEM((total, dc), BF16),
                pltpu.VMEM((total, dc), BF16),
                pltpu.VMEM((total, heads), BF16),
                pltpu.VMEM((2, total, hidden), F32),
                pltpu.VMEM((2, total, hidden), BF16),
                pltpu.VMEM((2, total, hidden), BF16),
                pltpu.VMEM((2, total, hidden), BF16),
                pltpu.VMEM((total, hidden), BF16),
                pltpu.VMEM((total, hidden), BF16),
                pltpu.VMEM((total, dc), BF16),
                pltpu.VMEM((n_tp, share, dc), BF16),
                pltpu.VMEM((n_tp, share, dc), BF16),
                pltpu.VMEM((share, dc), F32),
                pltpu.VMEM((n_fs, 8, rows_in), F32),
                pltpu.VMEM((n_fs, 8, share), F32),
                pltpu.VMEM((share, dc), BF16),
                pltpu.VMEM((rows_in, width), BF16),
                dma((7,)), dma((n_fs,)), dma((n_fs,)), dma((n_fs,)), dma((n_fs,)), dma((n_fs,)), dma((n_fs,)),
                dma((n_fs, 2)), dma((n_fs,)),
                dma((2, 2, n_chunks)), dma((2, 2, n_chunks)), dma((2, 2, n_chunks)), dma((2, 2, n_chunks)),
                dma((2, n_tp)), dma((2, n_tp)),
                dma((n_fs,)), dma((n_fs,)), dma((n_tp,)), dma((n_tp,)), dma((n_tp,)), dma((n_tp,)),
                dma((n_tp,)), dma((n_fs,)), dma((n_fs,)), dma((n_fs,)),
            ],
            compiler_params=pltpu.CompilerParams(
                collective_id=0, has_side_effects=True, vmem_limit_bytes=60 * 1024 * 1024),
        )(tokens, mix_heads, norm_first.reshape(1, -1), gate_first, up_first, down_first, out_weight,
          norm_second.reshape(1, -1), gate_second, up_second, down_second)

    in_specs = (
        P(("grp", "fs"), None),
        P(("grp", "fs"), "tp"),
        P(),
        P("fs", "tp"),
        P("fs", "tp"),
        P("tp", "fs"),
        P("tp", "fs"),
        P(),
        P("fs", "tp"),
        P("fs", "tp"),
        P("tp", "fs"),
    )
    return jax.shard_map(local, mesh=mesh, in_specs=in_specs, out_specs=P(("grp", "fs"), None), check_vma=False)
```

profile of v0, /device:TPU:0, one launch (start us, length us, event | category | flops | bytes accessed | tf_op | source)
XLA Modules:
  0.0 184.5 jit_solution(4681555206822394491)
XLA Ops:
  0.0 182.6 %shard_map.109 = bf16[128,2048]{1,0:T(8,128)(2,1)} custom-call(bf16[128,2048]{1,0:T(8,128)(2,1)} %tok.1, bf16[128,512]{1,0:T(8,128)(2,1)} %mix.1, f32[1,2048]{1,0:T(1,128)} %bitcast.2, bf16[512,1408]{1,0:T(8,128)(2,1)} %wg1.1, bf16[512,1408]{1,0:T(8,128)(2,1)} %wu1.1, bf16[1408,512]{1,0:T(8,128)(2,1)} %wd1.1, bf16[512,512]{1,0:T(8,128)(2,1)} %wo.1, ...), custom_call_target="tpu_custom_call" | custom-call | tf_op jit(solution)/shard_map/pallas_call | solution.py:478
  182.6 1.9 %copy.13 = bf16[128,2048]{1,0:T(8,128)(2,1)} copy(bf16[128,2048]{1,0:T(8,128)(2,1)} %shard_map.109) | data formatting | bytes 1048576
where the time goes:
time: 187 us; the launch traced here: 185 us
  Pallas kernels  183 us (98%)
  local copies, waits for them, and re-layouts  1.88 us (1%)
    pallas_call x1, Pallas kernels, local(): pl.pallas_call(functools.partial(kernel, n_fs, n_tp, chunk), out_shape=ja...  183 us

commit v1 on v0

--- a/solution.py
+++ b/solution.py
@@ -460,11 +460,582 @@
     loop(n_pairs, last_out)
 
 
+def by_count(counts, value, body):
+    for n in counts:
+        if len(counts) == 1:
+            body(n)
+        else:
+            pl.when(value == n)(functools.partial(body, n))
+
+
+def gathered(counts, n_fs, n_tp, n_q, lane,
+             tok, mix, gain1, wg1, wu1, wd1, wo, gain2, wg2, wu2, wd2,
+             out,
+             rows_of_me, wgu, wdb, wob, xs, mixed, hid, acc, part, r1, s1, r2, full, zs, rp, rr, zf, rf, resid, done, joined,
+             tok_sem, mix_sem, write_sem, wl_sem, dl_sem, wo_sem,
+             wz_send, wz_recv, wy_send, wy_recv, dz_send, dz_recv, dy_send, dy_recv,
+             ag_send, ag_recv, agr_send, ax_send, ax_recv, ad_send, ad_recv, af_send, af_recv,
+             mz_send, mz_recv, mr_send,
+             r1_send, r1_recv, r2_send, r2_recv, rp_send, rp_recv, rr_send, rr_recv, rf_send, rf_recv,
+             o_send, o_recv):
+    g, f, t = lax.axis_index("grp"), lax.axis_index("fs"), lax.axis_index("tp")
+    rows_in, width = tok.shape
+    dc, hidden = wg1.shape
+    n_x = n_tp // 2
+    core, x = t % 2, t // 2
+    sub = rows_in // n_tp
+    unit = n_fs * sub
+    u = core * n_x + x
+    u_x = core * n_x + 1 - x
+    u_pair = (1 - core) * n_x + x
+    u_diag = (1 - core) * n_x + 1 - x
+    t_x = (t + 2) % n_tp
+    t_pair = t + 1 - 2 * core
+    t_diag = (t_pair + 2) % n_tp
+    pair = f + 1 - 2 * (f % 2)
+    far0 = jnp.where(f < 2, 2, 0)
+    inner = jnp.logical_or(f == 1, f == 2)
+    bridge = jnp.where(f < 2, 2, 1)
+    others = (n_fs - 1 - f, (f + 2) % n_fs, pair)
+    n_k = 4
+    piece = dc // (2 * n_k)
+    qc = dc // n_q
+    n_lane = hidden // lane
+    most = max(counts)
+    gate_up = ((wg1, wu1), (wg2, wu2))
+    downs = (wd1, wd2)
+
+    def first(j):
+        return (j * n_lane + (1 - core) * (n_fs - 1)) // n_fs
+
+    def count(j):
+        return first(j + 1) - first(j)
+
+    mine = count(f)
+
+    def at(i, size):
+        return pl.ds(pl.multiple_of(i * size, size), size)
+
+    def remote(src, dst, send, recv, **where):
+        return pltpu.make_async_remote_copy(
+            src_ref=src, dst_ref=dst, send_sem=send, recv_sem=recv,
+            device_id=where, device_id_type=MESH)
+
+    def load_gate_up(n, l, m):
+        cols = pl.ds(pl.multiple_of(first(f) * lane, lane), n * lane)
+        return pltpu.make_async_copy(
+            gate_up[l][m].at[:, cols], wgu.at[l, m, at(f, dc), pl.ds(0, n * lane)], wl_sem.at[l, m])
+
+    def load_down(n, l, q):
+        rows = pl.ds(pl.multiple_of(first(f) * lane, lane), n * lane)
+        return pltpu.make_async_copy(
+            downs[l].at[rows, at(q, qc)], wdb.at[l, q, pl.ds(0, n * lane), at(f, qc)], dl_sem.at[l, q])
+
+    def start_loads(n):
+        for l in (0, 1):
+            for m in (0, 1):
+                load_gate_up(n, l, m).start()
+            for q in range(n_q):
+                load_down(n, l, q).start()
+        if n < most:
+            rest = pl.ds(n * lane, (most - n) * lane)
+            wgu[:, :, :, rest] = jnp.zeros((2, 2, width, (most - n) * lane), BF16)
+            wdb[:, :, rest, :] = jnp.zeros((2, n_q, (most - n) * lane, n_fs * qc), BF16)
+
+    barrier = pltpu.get_barrier_semaphore()
+    for i in range(n_fs - 1):
+        pl.semaphore_signal(barrier, inc=1, device_id={"fs": others[i]}, device_id_type=MESH)
+    pl.semaphore_signal(barrier, inc=1, device_id={"grp": 1 - g}, device_id_type=MESH)
+    for j in (t_x, t_pair, t_diag):
+        pl.semaphore_signal(barrier, inc=1, device_id={"tp": j}, device_id_type=MESH)
+
+    load_tok = pltpu.make_async_copy(tok, rows_of_me, tok_sem)
+    load_tok.start()
+    load_mix = [pltpu.make_async_copy(
+        mix.at[j * sub:(j + 1) * sub, :], mixed.at[(j % 2) * n_x + j // 2, f], mix_sem) for j in range(n_tp)]
+    for load in load_mix:
+        load.start()
+    by_count(counts, mine, start_loads)
+    load_out = pltpu.make_async_copy(wo, wob, wo_sem)
+    load_out.start()
+
+    def normed(values, gain):
+        squares = jnp.sum(values * values, axis=-1, keepdims=True)
+        return values * lax.rsqrt(squares * (1.0 / width) + EPS) * gain
+
+    load_tok.wait()
+    own = rows_of_me[at(t, sub), :].astype(F32)
+    xs[0, u, f] = normed(own, gain1[...]).astype(BF16)
+    for j in range(n_tp):
+        @pl.when(j != t)
+        def _():
+            rows = rows_of_me[j * sub:(j + 1) * sub, :].astype(F32)
+            xs[0, (j % 2) * n_x + j // 2, f] = normed(rows, gain1[...]).astype(BF16)
+    for q in range(n_q):
+        for j in range(n_fs):
+            resid[q, :, j * qc:(j + 1) * qc] = own[:, j * dc + q * qc:j * dc + (q + 1) * qc]
+    pltpu.make_async_copy(mixed.at[:, f], mixed.at[:, f], mix_sem).wait()
+    pl.semaphore_wait(barrier, n_fs - 1 + 1 + n_tp - 1)
+
+    def send_one(n, l, m, k, j):
+        cols = pl.ds(pl.multiple_of(first(j) * lane, lane), n * lane)
+        remote(gate_up[l][m].at[at(n_k * g + k, piece), cols],
+               wgu.at[l, m, at(n_k * (2 * f + g) + k, piece), pl.ds(0, n * lane)],
+               wz_send.at[l, j], wz_recv.at[l, m, k], fs=j).start()
+
+    def send_gate_up(l, r, where=others):
+        for j in where:
+            by_count(counts, count(j), lambda n, j=j: send_one(n, l, r % 2, r // 2, j))
+
+    def gate_up_y(n, l, m, k, j):
+        place = wgu.at[l, m, at(n_k * (2 * j + g) + k, piece), pl.ds(0, n * lane)]
+        return remote(place, place, wy_send.at[l], wy_recv.at[l, m, k], grp=1 - g)
+
+    def all_pieces(n, l, m, k, send, recv):
+        place = wgu.at[l, m, pl.ds(0, len(others) * piece), pl.ds(0, n * lane)]
+        return remote(place, place, send, recv, grp=1 - g)
+
+    def pass_gate_up(l, r):
+        m, k = r % 2, r // 2
+
+        def go(n):
+            all_pieces(n, l, m, k, wz_send.at[l, pair], wz_recv.at[l, m, k]).wait_recv()
+            for j in others:
+                gate_up_y(n, l, m, k, j).start()
+
+        by_count(counts, mine, go)
+
+    def take_gate_up(l, r):
+        m, k = r % 2, r // 2
+        by_count(counts, mine, lambda n: all_pieces(n, l, m, k, wy_send.at[l], wy_recv.at[l, m, k]).wait_recv())
+
+    def down_part(n, l, q, j, side):
+        size = n * lane // 2
+        return wdb.at[l, q, at(side, size), at(j, qc)]
+
+    def send_down(l, q, where=others):
+        for j in where:
+            def go(n, j=j):
+                size = n * lane // 2
+                rows = pl.ds(pl.multiple_of(first(j) * lane + g * size, lane // 2), size)
+                remote(downs[l].at[rows, at(q, qc)], down_part(n, l, q, f, g),
+                       dz_send.at[l, j], dz_recv.at[l, q, f], fs=j).start()
+
+            by_count(counts, count(j), go)
+
+    def down_y(n, l, q, j):
+        place = down_part(n, l, q, j, g)
+        return remote(place, place, dy_send.at[l], dy_recv.at[l, q], grp=1 - g)
+
+    def all_downs(n, l, q, send, recv):
+        place = wdb.at[l, q, pl.ds(0, n * lane // 2), pl.ds(0, len(others) * qc)]
+        return remote(place, place, send, recv, grp=1 - g)
+
+    def z_block(l, j, h, send, where):
+        place = xs.at[l, u, j, at(h, sub // 2)]
+        return remote(place, place, send, ag_recv.at[l, j, h], fs=where)
+
+    def x_block(l, j, who, h):
+        place = xs.at[l, who, j, at(h, sub // 2)]
+        return remote(place, place, ax_send.at[l], ax_recv.at[l, j, h], tp=t_x)
+
+    def pair_block(l, j, who, h):
+        place = xs.at[l, who, j, at(h, sub // 2)]
+        return remote(place, place, ad_send.at[l], ad_recv.at[l], tp=t_pair)
+
+    def diag_block(l, j, who, h):
+        place = xs.at[l, who, j, at(h, sub // 2)]
+        return remote(place, place, af_send.at[l], af_recv.at[l], tp=t_pair)
+
+    def pass_rows(l, j, h):
+        x_block(l, j, u, h).start()
+        pair_block(l, j, u, h).start()
+
+    def gather_own(l):
+        for h in (0, 1):
+            z_block(l, f, h, ag_send.at[l], bridge).start()
+        for h in (0, 1):
+            z_block(l, f, h, ag_send.at[l], pair).start()
+            if l == 1:
+                pass_rows(l, f, h)
+
+    def gather_near(l):
+        for h in (0, 1):
+            for k in (0, 1):
+                @pl.when(inner)
+                def _():
+                    j = far0 + k
+                    z_block(l, j, h, agr_send.at[l], j).wait_recv()
+                    z_block(l, j, h, agr_send.at[l], pair).start()
+                    pass_rows(l, j, h)
+
+        for h in (0, 1):
+            z_block(l, pair, h, ag_send.at[l], pair).wait_recv()
+            pass_rows(l, pair, h)
+
+    def gather_far(l):
+        for h in (0, 1):
+            for k in (0, 1):
+                @pl.when(jnp.logical_not(inner))
+                def _():
+                    j = far0 + k
+                    z_block(l, j, h, agr_send.at[l], j).wait_recv()
+                    pass_rows(l, j, h)
+
+    def gather_end(l):
+        blocks = [(j, h) for j in (far0, far0 + 1, pair) for h in (0, 1)]
+        if l == 1:
+            blocks = [(f, 0), (f, 1)] + blocks
+        for j, h in blocks:
+            x_block(l, j, u_x, h).wait_recv()
+            diag_block(l, j, u_x, h).start()
+        rows = xs.at[l, 0, pl.ds(0, len(blocks) // 2)]
+        remote(rows, rows, ad_send.at[l], ad_recv.at[l], tp=t_pair).wait_recv()
+        remote(rows, rows, af_send.at[l], af_recv.at[l], tp=t_pair).wait_recv()
+
+    def mix_block(j, send, where):
+        place = mixed.at[:, j]
+        return remote(place, place, send, mz_recv.at[j], fs=where)
+
+    def mix_near():
+        @pl.when(inner)
+        def _():
+            for k in (0, 1):
+                j = far0 + k
+                mix_block(j, mr_send.at[k], j).wait_recv()
+                mix_block(j, mr_send.at[k], pair).start()
+
+    def mix_far():
+        @pl.when(jnp.logical_not(inner))
+        def _():
+            for k in (0, 1):
+                mix_block(far0 + k, mr_send.at[k], far0 + k).wait_recv()
+
+        mix_block(pair, mz_send.at[1], pair).wait_recv()
+
+    def hidden_of(l):
+        def step(i):
+            rows = xs[l, at(i, n_x)].reshape(n_x * unit, width)
+            gate = jnp.dot(rows, wgu[l, 0], preferred_element_type=F32)
+            value = jnp.dot(rows, wgu[l, 1], preferred_element_type=F32)
+            hid[at(i, n_x * unit), :] = (gate / (1.0 + jnp.exp(-gate)) * value).astype(BF16)
+
+        loop(2, step)
+
+    def s1_copy(l, q):
+        return remote(part.at[l, q, at(1 - core, n_x)], r1.at[l, q], r1_send.at[l], r1_recv.at[l, q], tp=t_pair)
+
+    def s2_copy(l, q):
+        return remote(s1.at[l, q], r2.at[l, q], r2_send.at[l], r2_recv.at[l, q], tp=t_x)
+
+    def pair_copy(l, q):
+        return remote(zs.at[l, q, pair], rp.at[l, q], rp_send.at[l], rp_recv.at[l, q], fs=pair)
+
+    def relay_copy(l, q):
+        return remote(zs.at[l, q, pl.ds(far0, 2)], rr.at[l, q], rr_send.at[l], rr_recv.at[l, q], fs=pair)
+
+    def far_copy(l, q, k, where):
+        return remote(zf.at[l, q, k], rf.at[l, q], rf_send.at[l], rf_recv.at[l, q], fs=where)
+
+    def out_copy(q, where, who):
+        return remote(done.at[q], joined.at[q, at(who, sub)], o_send, o_recv.at[q], tp=where)
+
+    def pass_down(l, q):
+        def go(n):
+            for j in others:
+                place = down_part(n, l, q, j, g)
+                remote(place, place, dz_send.at[l, j], dz_recv.at[l, q, j], fs=j).wait_recv()
+                down_y(n, l, q, j).start()
+
+        by_count(counts, mine, go)
+
+    def write_copy(q, j):
+        return pltpu.make_async_copy(
+            joined.at[q, :, at(j, qc)], out.at[:, pl.ds(pl.multiple_of(j * dc + q * qc, qc), qc)], write_sem)
+
+    def reduced(l, hooks):
+        def multiply(q):
+            @pl.when(q < n_q - 1)
+            def _():
+                pass_down(l, q + 1)
+
+            def ready(n):
+                all_downs(n, l, q, dy_send.at[l], dy_recv.at[l, q]).wait_recv()
+                load_down(n, l, q).wait()
+
+            by_count(counts, mine, ready)
+
+            def side(i):
+                c = (1 - core) * (1 - i) + core * i
+                value = 0.5 * jnp.dot(hid[at(c, n_x * unit), :], wdb[l, q], preferred_element_type=F32)
+                if l == 0:
+                    acc[...] = value
+                    heads = mixed[at(c, n_x)].reshape(n_x * unit, mixed.shape[-1])
+                    acc[:, at(f, qc)] = acc[:, at(f, qc)] + jnp.dot(
+                        heads, wob[:, at(q, qc)], preferred_element_type=F32)
+                    value = acc[...]
+                part[l, q, at(c, n_x)] = value.astype(BF16).reshape(n_x, n_fs, sub, n_fs * qc)
+
+                @pl.when(i == 0)
+                def _():
+                    s1_copy(l, q).start()
+
+            loop(2, side)
+
+        def across(q):
+            s1_copy(l, q).wait_recv()
+            s1[l, q] = (part[l, q, u_x].astype(F32) + r1[l, q, 1 - x].astype(F32)).astype(BF16)
+            s2_copy(l, q).start()
+
+        def along(q):
+            s2_copy(l, q).wait_recv()
+            value = part[l, q, u].astype(F32) + r1[l, q, x].astype(F32) + r2[l, q].astype(F32)
+            full[l, q] = value
+            zs[l, q] = value.astype(BF16)
+
+            @pl.when(jnp.logical_not(inner))
+            def _():
+                relay_copy(l, q).start()
+
+            pair_copy(l, q).start()
+
+        def relay(q):
+            @pl.when(inner)
+            def _():
+                relay_copy(l, q).wait_recv()
+                for k in (0, 1):
+                    zf[l, q, k] = (full[l, q, far0 + k] + rr[l, q, k].astype(F32)).astype(BF16)
+                    far_copy(l, q, k, far0 + k).start()
+
+        def finish(q):
+            pair_copy(l, q).wait_recv()
+            far_copy(l, q, 0, far0).wait_recv()
+            value = full[l, q, f] + rp[l, q].astype(F32) + rf[l, q].astype(F32)
+            value = resid[q] + value
+            if l == 0:
+                resid[q] = value
+            else:
+                done[q] = value.astype(BF16)
+                joined[q, at(t, sub)] = value.astype(BF16)
+                for where in (t_x, t_diag, t_pair):
+                    out_copy(q, where, t).start()
+
+        def write(q):
+            rows = joined.at[q, pl.ds(0, (n_tp - 1) * sub)]
+            remote(rows, rows, o_send, o_recv.at[q], tp=t_pair).wait_recv()
+            for j in range(n_fs):
+                write_copy(q, j).start()
+
+        stages = [(multiply, 0), (across, 0), (along, 1), (relay, 2), (finish, 4 - l)]
+        if l == 1:
+            stages.append((write, 4))
+
+        def step(s):
+            for stage, lag in stages:
+                @pl.when(jnp.logical_and(s >= lag, s < n_q + lag))
+                def _():
+                    stage(s - lag)
+
+            for when, hook in hooks:
+                pl.when(s == when)(hook)
+
+        loop(n_q + stages[-1][1], step)
+
+    def sent(ref, sem):
+        remote(ref, ref, sem, ag_recv.at[0, 0, 0], tp=t_pair).wait_send()
+
+    def drain_gate_up(l):
+        for j in others:
+            by_count(counts, count(j), lambda n, j=j: sent(
+                wgu.at[l, 0, pl.ds(0, dc), pl.ds(0, n * lane)], wz_send.at[l, j]))
+        by_count(counts, mine, lambda n: sent(
+            wgu.at[l, 0, pl.ds(0, len(others) * dc), pl.ds(0, n * lane)], wy_send.at[l]))
+        sent(xs.at[l, 0, pl.ds(0, 2)], ag_send.at[l])
+        pl.when(inner)(lambda: sent(xs.at[l, 0, pl.ds(0, 2)], agr_send.at[l]))
+        rows = xs.at[l, 0, pl.ds(0, 4 if l == 1 else 3)]
+        for sem in (ax_send, ad_send, af_send):
+            sent(rows, sem.at[l])
+
+    def drain_mix():
+        mix_block(f, mz_send.at[0], bridge).wait_send()
+        mix_block(f, mz_send.at[1], pair).wait_send()
+
+        @pl.when(inner)
+        def _():
+            for k in (0, 1):
+                mix_block(far0 + k, mr_send.at[k], pair).wait_send()
+
+    def drain_down(l):
+        for j in others:
+            by_count(counts, count(j), lambda n, j=j: sent(
+                wdb.at[l, 0, pl.ds(0, n * lane // 2)], dz_send.at[l, j]))
+        by_count(counts, mine, lambda n: sent(
+            wdb.at[l, pl.ds(0, len(others)), pl.ds(0, n * lane // 2)], dy_send.at[l]))
+
+    def drain_steps(l):
+        sent(part.at[l, :, pl.ds(0, n_x)], r1_send.at[l])
+        sent(s1.at[l], r2_send.at[l])
+        sent(zs.at[l, 0], rp_send.at[l])
+        pl.when(inner)(lambda: sent(zs.at[l, pl.ds(0, 2)], rf_send.at[l]))
+        pl.when(jnp.logical_not(inner))(lambda: sent(zs.at[l, pl.ds(0, 2)], rr_send.at[l]))
+        if l == 1:
+            sent(joined.at[:, pl.ds(0, (n_tp - 1) * sub)], o_send)
+
+    def wait_own(l):
+        for m in (0, 1):
+            by_count(counts, mine, lambda n, m=m: load_gate_up(n, l, m).wait())
+
+    def mix_own():
+        mix_block(f, mz_send.at[0], bridge).start()
+        mix_block(f, mz_send.at[1], pair).start()
+
+    items = (
+        *(functools.partial(send_gate_up, 0, r) for r in range(8)), mix_own,
+        *(functools.partial(send_down, 0, q) for q in range(n_q)),
+        *(functools.partial(send_gate_up, 1, r) for r in range(8)),
+        *(functools.partial(send_down, 1, q) for q in range(n_q)))
+    inner_plan = (13, 13, 13, 13, 13, 13, 13, 13, 13, 15, 16, 17, 18, 19, 20, 21, 21, 21, 21, 22, 23, 24, 25)
+    outer_plan = (9, 10, 11, 12, 13, 13, 13, 13, 13, 14, 15, 16, 17, 18, 19, 20, 20, 20, 20, 21, 22, 23, 25)
+    pass_plan = (0, 0, 0, 0, 0, 0, 0, 0, 0, 0, 0, 0, 0, 1, 2, 3, 4, 5, 6, 7, 8, 8, 8)
+
+    def point(p):
+        for plan, mask in ((inner_plan, inner), (outer_plan, jnp.logical_not(inner))):
+            group = items[plan[p - 1] if p else 0:plan[p]]
+            if group:
+                @pl.when(mask)
+                def _():
+                    for item in group:
+                        item()
+        for r in range(pass_plan[p - 1] if p else 0, pass_plan[p]):
+            pass_gate_up(1, r)
+
+    gather_own(0)
+    point(0)
+    gather_near(0)
+    for r in range(8):
+        pass_gate_up(0, r)
+        point(r + 1)
+        if r == 0:
+            gather_far(0)
+        if r == 3:
+            gather_end(0)
+    mix_near()
+    point(9)
+    pass_down(0, 0)
+    wait_own(0)
+    load_out.wait()
+    for r in range(8):
+        take_gate_up(0, r)
+    hidden_of(0)
+    point(10)
+    mix_far()
+    reduced(0, tuple((k, functools.partial(point, 11 + k)) for k in range(8)))
+
+    squares = jnp.sum(resid[0] * resid[0], axis=-1, keepdims=True)
+    for q in range(1, n_q):
+        squares = squares + jnp.sum(resid[q] * resid[q], axis=-1, keepdims=True)
+    scale = lax.rsqrt(squares * (1.0 / width) + EPS)
+    for q in range(n_q):
+        for j in range(n_fs):
+            cols = slice(j * dc + q * qc, j * dc + (q + 1) * qc)
+            xs[1, u, f, :, cols] = (resid[q, :, j * qc:(j + 1) * qc] * scale * gain2[:, cols]).astype(BF16)
+
+    gather_own(1)
+    point(19)
+    gather_near(1)
+    point(20)
+    gather_far(1)
+    point(21)
+    drain_gate_up(0)
+    drain_mix()
+    gather_end(1)
+    point(22)
+    drain_down(0)
+    drain_steps(0)
+    pass_down(1, 0)
+    wait_own(1)
+    for r in range(8):
+        take_gate_up(1, r)
+    hidden_of(1)
+    reduced(1, ((2, functools.partial(drain_gate_up, 1)), (4, functools.partial(drain_down, 1))))
+    drain_steps(1)
+
+    pltpu.make_async_copy(joined, joined, write_sem).wait()
+
+
+def gathered_call(mesh, args):
+    n_fs, n_tp = mesh.shape["fs"], mesh.shape["tp"]
+    tokens, mix_heads, _, gate_first = args[:4]
+    rows_in, width = tokens.shape
+    dc, hidden = gate_first.shape
+    heads = mix_heads.shape[1]
+    lane, n_q = 128, dc // 128
+    n_lane = hidden // lane
+    counts = sorted({-(-(j + 1) * n_lane // n_fs) - -(-j * n_lane // n_fs) for j in range(n_fs)})
+    most = counts[-1] * lane
+    sub, total, qc = rows_in // n_tp, rows_in * n_fs, dc // n_q
+    n_x, wide = n_tp // 2, n_fs * qc
+    dma = pltpu.SemaphoreType.DMA
+    vmem = pl.BlockSpec(memory_space=pltpu.VMEM)
+    hbm = pl.BlockSpec(memory_space=pl.ANY)
+    lq = (2, n_q)
+    return pl.pallas_call(
+        functools.partial(gathered, counts, n_fs, n_tp, n_q, lane),
+        out_shape=jax.ShapeDtypeStruct((rows_in, width), BF16),
+        in_specs=[hbm, hbm, vmem, hbm, hbm, hbm, hbm, vmem, hbm, hbm, hbm],
+        out_specs=hbm,
+        scratch_shapes=[
+            pltpu.VMEM((rows_in, width), BF16),
+            pltpu.VMEM((2, 2, width, most), BF16),
+            pltpu.VMEM((2, n_q, most, wide), BF16),
+            pltpu.VMEM((heads, dc), BF16),
+            pltpu.VMEM((2, n_tp, n_fs, sub, width), BF16),
+            pltpu.VMEM((n_tp, n_fs, sub, heads), BF16),
+            pltpu.VMEM((total, most), BF16),
+            pltpu.VMEM((total // 2, wide), F32),
+            pltpu.VMEM((*lq, n_tp, n_fs, sub, wide), BF16),
+            pltpu.VMEM((*lq, n_x, n_fs, sub, wide), BF16),
+            pltpu.VMEM((*lq, n_fs, sub, wide), BF16),
+            pltpu.VMEM((*lq, n_fs, sub, wide), BF16),
+            pltpu.VMEM((*lq, n_fs, sub, wide), F32),
+            pltpu.VMEM((*lq, n_fs, sub, wide), BF16),
+            pltpu.VMEM((*lq, sub, wide), BF16),
+            pltpu.VMEM((*lq, 2, sub, wide), BF16),
+            pltpu.VMEM((*lq, 2, sub, wide), BF16),
+            pltpu.VMEM((*lq, sub, wide), BF16),
+            pltpu.VMEM((n_q, sub, wide), F32),
+            pltpu.VMEM((n_q, sub, wide), BF16),
+            pltpu.VMEM((n_q, rows_in, wide), BF16),
+            dma, dma, dma, dma((2, 2)), dma(lq), dma,
+            dma((2, n_fs)), dma((2, 2, 4)), dma((2,)), dma((2, 2, 4)),
+            dma((2, n_fs)), dma((*lq, n_fs)), dma((2,)), dma(lq),
+            dma((2,)), dma((2, n_fs, 2)), dma((2,)),
+            dma((2,)), dma((2, n_fs, 2)), dma((2,)), dma((2,)), dma((2,)), dma((2,)),
+            dma((2,)), dma((n_fs,)), dma((2,)),
+            *[dma((2,)), dma(lq)] * 5,
+            dma, dma((n_q,)),
+        ],
+        compiler_params=pltpu.CompilerParams(
+            collective_id=0, has_side_effects=True, vmem_limit_bytes=60 * 1024 * 1024),
+    )(*args)
+
+
+def fits(mesh, args):
+    tokens, gate = args[0], args[3]
+    n_tp = mesh.shape["tp"]
+    return (mesh.shape["grp"] == 2 and mesh.shape["fs"] == 4 and n_tp == 4 and tokens.shape[0] % (32 * n_tp) == 0
+            and gate.shape[0] % 512 == 0 and gate.shape[1] % 128 == 0)
+
+
 def solution(mesh):
     n_fs, n_tp = mesh.shape["fs"], mesh.shape["tp"]
 
     def local(tokens, mix_heads, norm_first, gate_first, up_first, down_first, out_weight,
               norm_second, gate_second, up_second, down_second):
+        args = (tokens, mix_heads, norm_first.reshape(1, -1), gate_first, up_first, down_first, out_weight,
+                norm_second.reshape(1, -1), gate_second, up_second, down_second)
+        if fits(mesh, args):
+            return gathered_call(mesh, args)
         rows_in, width = tokens.shape
         total = rows_in * n_fs
         share = total // n_tp
@@ -514,8 +1085,7 @@
             ],
             compiler_params=pltpu.CompilerParams(
                 collective_id=0, has_side_effects=True, vmem_limit_bytes=60 * 1024 * 1024),
-        )(tokens, mix_heads, norm_first.reshape(1, -1), gate_first, up_first, down_first, out_weight,
-          norm_second.reshape(1, -1), gate_second, up_second, down_second)
+        )(*args)
 
     in_specs = (
         P(("grp", "fs"), None),

time: 187 us -> 156 us (0.83)
  Pallas kernels: 183 us -> 152 us
    pallas_call x1, Pallas kernels: 183 us -> 152 us  [gathered_call(): pl.pallas_call(functools.partial(gathered, counts, n_fs, n_tp, n_q, lane)...]
where the time goes in v1:
time: 156 us; the launch traced here: 154 us
  Pallas kernels  152 us (97%)
  local copies, waits for them, and re-layouts  1.88 us (1%)
    pallas_call x1, Pallas kernels, gathered_call(): pl.pallas_call(functools.partial(gathered, counts, n_fs, n_tp, n_q, lane)...  152 us

profile of v1, /device:TPU:0, one launch (start us, length us, event | category | flops | bytes accessed | tf_op | source)
XLA Modules:
  0.0 154.2 jit_solution(17433974035527452242)
XLA Ops:
  0.0 152.3 %shard_map.109 = bf16[128,2048]{1,0:T(8,128)(2,1)} custom-call(bf16[128,2048]{1,0:T(8,128)(2,1)} %tok.1, bf16[128,512]{1,0:T(8,128)(2,1)} %mix.1, f32[1,2048]{1,0:T(1,128)} %bitcast.2, bf16[512,1408]{1,0:T(8,128)(2,1)} %wg1.1, bf16[512,1408]{1,0:T(8,128)(2,1)} %wu1.1, bf16[1408,512]{1,0:T(8,128)(2,1)} %wd1.1, bf16[512,512]{1,0:T(8,128)(2,1)} %wo.1, ...), custom_call_target="tpu_custom_call" | custom-call | tf_op jit(solution)/shard_map/pallas_call | solution.py:982
  152.4 1.9 %copy.13 = bf16[128,2048]{1,0:T(8,128)(2,1)} copy(bf16[128,2048]{1,0:T(8,128)(2,1)} %shard_map.109) | data formatting | bytes 1048576

commit v2 on v1

--- a/solution.py
+++ b/solution.py
@@ -471,12 +471,12 @@
 def gathered(counts, n_fs, n_tp, n_q, lane,
              tok, mix, gain1, wg1, wu1, wd1, wo, gain2, wg2, wu2, wd2,
              out,
-             rows_of_me, wgu, wdb, wob, xs, mixed, hid, acc, part, r1, s1, r2, full, zs, rp, rr, zf, rf, resid, done, joined,
+             rows_of_me, wgu, wdb, wob, xs, mixed, hid, acc, part, r1, s1, r2, full, zs, rp, rr, zf, rf, rg, resid, done, joined,
              tok_sem, mix_sem, write_sem, wl_sem, dl_sem, wo_sem,
              wz_send, wz_recv, wy_send, wy_recv, dz_send, dz_recv, dy_send, dy_recv,
              ag_send, ag_recv, agr_send, ax_send, ax_recv, ad_send, ad_recv, af_send, af_recv,
              mz_send, mz_recv, mr_send,
-             r1_send, r1_recv, r2_send, r2_recv, rp_send, rp_recv, rr_send, rr_recv, rf_send, rf_recv,
+             r1_send, r1_recv, r2_send, r2_recv, rp_send, rp_recv, rr_send, rr_recv, rf_send, rf_recv, rg_send, rg_recv,
              o_send, o_recv):
     g, f, t = lax.axis_index("grp"), lax.axis_index("fs"), lax.axis_index("tp")
     rows_in, width = tok.shape
@@ -496,7 +496,7 @@
     far0 = jnp.where(f < 2, 2, 0)
     inner = jnp.logical_or(f == 1, f == 2)
     bridge = jnp.where(f < 2, 2, 1)
-    others = (n_fs - 1 - f, (f + 2) % n_fs, pair)
+    others = (jnp.where(f < 2, n_fs - 1, 0), bridge, pair)
     n_k = 4
     piece = dc // (2 * n_k)
     qc = dc // n_q
@@ -731,11 +731,17 @@
     def pair_copy(l, q):
         return remote(zs.at[l, q, pair], rp.at[l, q], rp_send.at[l], rp_recv.at[l, q], fs=pair)
 
-    def relay_copy(l, q):
-        return remote(zs.at[l, q, pl.ds(far0, 2)], rr.at[l, q], rr_send.at[l], rr_recv.at[l, q], fs=pair)
-
-    def far_copy(l, q, k, where):
-        return remote(zf.at[l, q, k], rf.at[l, q], rf_send.at[l], rf_recv.at[l, q], fs=where)
+    def relay_copy(q):
+        return remote(zs.at[0, q, pl.ds(far0, 2)], rr.at[q], rr_send, rr_recv.at[q], fs=pair)
+
+    def far_copy(q, k, where):
+        return remote(zf.at[q, k], rf.at[0, q], rf_send.at[0], rf_recv.at[0, q], fs=where)
+
+    def straight(q, k, where):
+        return remote(zs.at[1, q, far0 + k], rg.at[q], rg_send, rg_recv.at[q], fs=where)
+
+    def straight_inner(q, k, where):
+        return remote(zs.at[1, q, far0 + k], rf.at[1, q], rf_send.at[1], rf_recv.at[1, q], fs=where)
 
     def out_copy(q, where, who):
         return remote(done.at[q], joined.at[q, at(who, sub)], o_send, o_recv.at[q], tp=where)
@@ -793,25 +799,39 @@
             full[l, q] = value
             zs[l, q] = value.astype(BF16)
 
-            @pl.when(jnp.logical_not(inner))
-            def _():
-                relay_copy(l, q).start()
+            if l == 0:
+                pl.when(jnp.logical_not(inner))(lambda: relay_copy(q).start())
+            else:
+                @pl.when(inner)
+                def _():
+                    for k in (0, 1):
+                        straight_inner(q, k, far0 + k).start()
+
+                @pl.when(jnp.logical_not(inner))
+                def _():
+                    for k in (0, 1):
+                        straight(q, k, far0 + k).start()
 
             pair_copy(l, q).start()
 
         def relay(q):
             @pl.when(inner)
             def _():
-                relay_copy(l, q).wait_recv()
+                relay_copy(q).wait_recv()
                 for k in (0, 1):
-                    zf[l, q, k] = (full[l, q, far0 + k] + rr[l, q, k].astype(F32)).astype(BF16)
-                    far_copy(l, q, k, far0 + k).start()
+                    zf[q, k] = (full[0, q, far0 + k] + rr[q, k].astype(F32)).astype(BF16)
+                    far_copy(q, k, far0 + k).start()
 
         def finish(q):
             pair_copy(l, q).wait_recv()
-            far_copy(l, q, 0, far0).wait_recv()
-            value = full[l, q, f] + rp[l, q].astype(F32) + rf[l, q].astype(F32)
-            value = resid[q] + value
+            value = full[l, q, f] + rp[l, q].astype(F32)
+            if l == 0:
+                far_copy(q, 0, far0).wait_recv()
+            else:
+                straight_inner(q, 0, far0).wait_recv()
+                straight(q, 0, far0).wait_recv()
+                value = value + rg[q].astype(F32)
+            value = resid[q] + (value + rf[l, q].astype(F32))
             if l == 0:
                 resid[q] = value
             else:
@@ -826,9 +846,8 @@
             for j in range(n_fs):
                 write_copy(q, j).start()
 
-        stages = [(multiply, 0), (across, 0), (along, 1), (relay, 2), (finish, 4 - l)]
-        if l == 1:
-            stages.append((write, 4))
+        stages = [(multiply, 0), (across, 0), (along, 1)]
+        stages += [(relay, 2), (finish, 4)] if l == 0 else [(finish, 2), (write, 3)]
 
         def step(s):
             for stage, lag in stages:
@@ -877,7 +896,7 @@
         sent(s1.at[l], r2_send.at[l])
         sent(zs.at[l, 0], rp_send.at[l])
         pl.when(inner)(lambda: sent(zs.at[l, pl.ds(0, 2)], rf_send.at[l]))
-        pl.when(jnp.logical_not(inner))(lambda: sent(zs.at[l, pl.ds(0, 2)], rr_send.at[l]))
+        pl.when(jnp.logical_not(inner))(lambda: sent(zs.at[l, pl.ds(0, 2)], rg_send if l else rr_send))
         if l == 1:
             sent(joined.at[:, pl.ds(0, (n_tp - 1) * sub)], o_send)
 
@@ -885,27 +904,34 @@
         for m in (0, 1):
             by_count(counts, mine, lambda n, m=m: load_gate_up(n, l, m).wait())
 
-    def mix_own():
-        mix_block(f, mz_send.at[0], bridge).start()
-        mix_block(f, mz_send.at[1], pair).start()
-
-    items = (
-        *(functools.partial(send_gate_up, 0, r) for r in range(8)), mix_own,
+    cross, near = others[:2], others[2:]
+
+    def mix_to(where):
+        if where is not near:
+            mix_block(f, mz_send.at[0], bridge).start()
+        if where is not cross:
+            mix_block(f, mz_send.at[1], pair).start()
+
+    items = [
+        *(functools.partial(send_gate_up, 0, r) for r in range(8)),
         *(functools.partial(send_down, 0, q) for q in range(n_q)),
         *(functools.partial(send_gate_up, 1, r) for r in range(8)),
-        *(functools.partial(send_down, 1, q) for q in range(n_q)))
-    inner_plan = (13, 13, 13, 13, 13, 13, 13, 13, 13, 15, 16, 17, 18, 19, 20, 21, 21, 21, 21, 22, 23, 24, 25)
-    outer_plan = (9, 10, 11, 12, 13, 13, 13, 13, 13, 14, 15, 16, 17, 18, 19, 20, 20, 20, 20, 21, 22, 23, 25)
+        *(functools.partial(send_down, 1, q) for q in range(n_q))]
+    items.insert(5, mix_to)
+    plans = (
+        (inner, cross, (13, 13, 13, 13, 13, 13, 13, 13, 13, 15, 16, 17, 18, 19, 20, 21, 21, 21, 21, 22, 23, 24, 25)),
+        (inner, near, (13, 13, 13, 13, 13, 13, 13, 13, 13, 15, 16, 17, 18, 19, 20, 21, 21, 21, 21, 22, 23, 24, 25)),
+        (jnp.logical_not(inner), others, (9, 10, 11, 12, 13, 13, 13, 13, 13, 14, 15, 16, 17, 18, 19, 20, 20, 20, 20, 21, 22, 23, 25)))
     pass_plan = (0, 0, 0, 0, 0, 0, 0, 0, 0, 0, 0, 0, 0, 1, 2, 3, 4, 5, 6, 7, 8, 8, 8)
 
     def point(p):
-        for plan, mask in ((inner_plan, inner), (outer_plan, jnp.logical_not(inner))):
+        for mask, where, plan in plans:
             group = items[plan[p - 1] if p else 0:plan[p]]
             if group:
                 @pl.when(mask)
                 def _():
                     for item in group:
-                        item()
+                        item(where)
         for r in range(pass_plan[p - 1] if p else 0, pass_plan[p]):
             pass_gate_up(1, r)
 
@@ -915,11 +941,14 @@
     for r in range(8):
         pass_gate_up(0, r)
         point(r + 1)
+        if r == 6:
+            mix_near()
         if r == 0:
             gather_far(0)
         if r == 3:
             gather_end(0)
-    mix_near()
+    if 6 == 8:
+        mix_near()
     point(9)
     pass_down(0, 0)
     wait_own(0)
@@ -969,7 +998,7 @@
     rows_in, width = tokens.shape
     dc, hidden = gate_first.shape
     heads = mix_heads.shape[1]
-    lane, n_q = 128, dc // 128
+    lane, n_q = 128, n_fs
     n_lane = hidden // lane
     counts = sorted({-(-(j + 1) * n_lane // n_fs) - -(-j * n_lane // n_fs) for j in range(n_fs)})
     most = counts[-1] * lane
@@ -1000,9 +1029,10 @@
             pltpu.VMEM((*lq, n_fs, sub, wide), F32),
             pltpu.VMEM((*lq, n_fs, sub, wide), BF16),
             pltpu.VMEM((*lq, sub, wide), BF16),
-            pltpu.VMEM((*lq, 2, sub, wide), BF16),
-            pltpu.VMEM((*lq, 2, sub, wide), BF16),
+            pltpu.VMEM((n_q, 2, sub, wide), BF16),
+            pltpu.VMEM((n_q, 2, sub, wide), BF16),
             pltpu.VMEM((*lq, sub, wide), BF16),
+            pltpu.VMEM((n_q, sub, wide), BF16),
             pltpu.VMEM((n_q, sub, wide), F32),
             pltpu.VMEM((n_q, sub, wide), BF16),
             pltpu.VMEM((n_q, rows_in, wide), BF16),
@@ -1012,7 +1042,7 @@
             dma((2,)), dma((2, n_fs, 2)), dma((2,)),
             dma((2,)), dma((2, n_fs, 2)), dma((2,)), dma((2,)), dma((2,)), dma((2,)),
             dma((2,)), dma((n_fs,)), dma((2,)),
-            *[dma((2,)), dma(lq)] * 5,
+            *[dma((2,)), dma(lq)] * 3, dma, dma((n_q,)), dma((2,)), dma(lq), dma, dma((n_q,)),
             dma, dma((n_q,)),
         ],
         compiler_params=pltpu.CompilerParams(
@@ -1024,7 +1054,7 @@
     tokens, gate = args[0], args[3]
     n_tp = mesh.shape["tp"]
     return (mesh.shape["grp"] == 2 and mesh.shape["fs"] == 4 and n_tp == 4 and tokens.shape[0] % (32 * n_tp) == 0
-            and gate.shape[0] % 512 == 0 and gate.shape[1] % 128 == 0)
+            and gate.shape[0] % (128 * 4) == 0 and gate.shape[1] % 128 == 0)
 
 
 def solution(mesh):

time: 156 us -> 152 us (0.974)
  Pallas kernels: 152 us -> 150 us
    pallas_call x1, Pallas kernels: 152 us -> 150 us  [gathered_call(): pl.pallas_call(functools.partial(gathered, counts, n_fs, n_tp, n_q, lane)...]
where the time goes in v2:
time: 152 us
  Pallas kernels  150 us (99%)
  local copies, waits for them, and re-layouts  1.88 us (1%)
    pallas_call x1, Pallas kernels, gathered_call(): pl.pallas_call(functools.partial(gathered, counts, n_fs, n_tp, n_q, lane)...  150 us

profile of v2, /device:TPU:0, one launch (start us, length us, event | category | flops | bytes accessed | tf_op | source)
XLA Modules:
  0.0 151.7 jit_solution(6209841135123979730)
XLA Ops:
  0.0 149.8 %shard_map.109 = bf16[128,2048]{1,0:T(8,128)(2,1)} custom-call(bf16[128,2048]{1,0:T(8,128)(2,1)} %tok.1, bf16[128,512]{1,0:T(8,128)(2,1)} %mix.1, f32[1,2048]{1,0:T(1,128)} %bitcast.2, bf16[512,1408]{1,0:T(8,128)(2,1)} %wg1.1, bf16[512,1408]{1,0:T(8,128)(2,1)} %wu1.1, bf16[1408,512]{1,0:T(8,128)(2,1)} %wd1.1, bf16[512,512]{1,0:T(8,128)(2,1)} %wo.1, ...), custom_call_target="tpu_custom_call" | custom-call | tf_op jit(solution)/shard_map/pallas_call | solution.py:1011
  149.9 1.9 %copy.13 = bf16[128,2048]{1,0:T(8,128)(2,1)} copy(bf16[128,2048]{1,0:T(8,128)(2,1)} %shard_map.109) | data formatting | bytes 1048576

commit v3 on v2

--- a/solution.py
+++ b/solution.py
@@ -919,10 +919,10 @@
         *(functools.partial(send_down, 1, q) for q in range(n_q))]
     items.insert(5, mix_to)
     plans = (
-        (inner, cross, (13, 13, 13, 13, 13, 13, 13, 13, 13, 15, 16, 17, 18, 19, 20, 21, 21, 21, 21, 22, 23, 24, 25)),
-        (inner, near, (13, 13, 13, 13, 13, 13, 13, 13, 13, 15, 16, 17, 18, 19, 20, 21, 21, 21, 21, 22, 23, 24, 25)),
+        (inner, cross, (13, 13, 13, 13, 13, 13, 13, 13, 13, 15, 16, 17, 18, 19, 20, 21, 21, 21, 21, 21, 22, 24, 25)),
+        (inner, near, (13, 13, 13, 13, 13, 13, 13, 13, 13, 15, 16, 17, 18, 19, 20, 21, 21, 21, 21, 21, 22, 24, 25)),
         (jnp.logical_not(inner), others, (9, 10, 11, 12, 13, 13, 13, 13, 13, 14, 15, 16, 17, 18, 19, 20, 20, 20, 20, 21, 22, 23, 25)))
-    pass_plan = (0, 0, 0, 0, 0, 0, 0, 0, 0, 0, 0, 0, 0, 1, 2, 3, 4, 5, 6, 7, 8, 8, 8)
+    pass_plan = (0, 0, 0, 0, 0, 0, 0, 0, 0, 0, 0, 0, 0, 1, 2, 3, 4, 5, 6, 6, 7, 8, 8)
 
     def point(p):
         for mask, where, plan in plans:

time: 152 us -> 152 us (level)
  no operation moved by 1% of the time
where the time goes in v3:
time: 152 us
  Pallas kernels  150 us (99%)
  local copies, waits for them, and re-layouts  1.88 us (1%)
    pallas_call x1, Pallas kernels, gathered_call(): pl.pallas_call(functools.partial(gathered, counts, n_fs, n_tp, n_q, lane)...  150 us

profile of v3, /device:TPU:0, one launch (start us, length us, event | category | flops | bytes accessed | tf_op | source)
XLA Modules:
  0.0 151.8 jit_solution(12291774385450882860)
XLA Ops:
  0.0 149.9 %shard_map.109 = bf16[128,2048]{1,0:T(8,128)(2,1)} custom-call(bf16[128,2048]{1,0:T(8,128)(2,1)} %tok.1, bf16[128,512]{1,0:T(8,128)(2,1)} %mix.1, f32[1,2048]{1,0:T(1,128)} %bitcast.2, bf16[512,1408]{1,0:T(8,128)(2,1)} %wg1.1, bf16[512,1408]{1,0:T(8,128)(2,1)} %wu1.1, bf16[1408,512]{1,0:T(8,128)(2,1)} %wd1.1, bf16[512,512]{1,0:T(8,128)(2,1)} %wo.1, ...), custom_call_target="tpu_custom_call" | custom-call | tf_op jit(solution)/shard_map/pallas_call | solution.py:1011
  149.9 1.9 %copy.13 = bf16[128,2048]{1,0:T(8,128)(2,1)} copy(bf16[128,2048]{1,0:T(8,128)(2,1)} %shard_map.109) | data formatting | bytes 1048576
